TPU v7x, 32 devices: a whole 2x2x4 slice. The times are simulated.
32 devices in a mesh: grp: 2 (over y), fs: 4 (over z), tp: 4 (over x, core).
Axes of the slice: x: 2, y: 2, z: 4, core: 2. Of those that a mesh axis runs over, the one named last changes fastest.
Arguments:
- stream: bfloat16 [8, 128, 2048], P(('grp', 'fs')), parts along dimension 0, may hold values from -6 to 6
- in_gain: float32 [2048], replicated, may hold values from 0.2 to 5
- value_weight: bfloat16 [2048, 1024], P('fs', 'tp'), may hold values from -0.125 to 0.125
- gate_weight: bfloat16 [2048, 1024], P('fs', 'tp'), may hold values from -0.125 to 0.125
- conv_kernel: bfloat16 [31, 1024], P(None, 'tp'), may hold values from -3.6 to 3.6
- conv_gain: float32 [1024], P('tp'), may hold values from 0.1 to 1.9
- conv_shift: float32 [1024], P('tp'), may hold values from -3 to 3
- out_weight: bfloat16 [1024, 2048], P('tp', 'fs'), may hold values from -0.1875 to 0.1875
- norm_gain: float32 [2048], replicated, may hold values from 0.2 to 5
- up_weight: bfloat16 [2048, 8192], P('fs', 'tp'), may hold values from -0.125 to 0.125
- down_weight: bfloat16 [8192, 2048], P('tp', 'fs'), may hold values from -0.0625 to 0.0625
- out_gain: float32 [2048], P('tp'), may hold values from 0.1 to 1.9
Outputs:
- result: bfloat16 [8, 128, 2048], P(('grp', 'fs'), None, 'tp'), parts along dimension 0
There are 2 independent parts, one for each index of `grp`. A program takes and returns all parts, laid end to end along the dimension named above; an argument that names none is the same for every part. Nothing has to cross between parts.
All inputs are finite; a program needn't handle non-finite values.
Results may differ from a plain program's by a relative error of at most 0.02.
Values may be sent and summed in bfloat16 or wider, within the bound.
A program may use at most 64 MiB of HBM per device.

v0:
```python
import jax
import jax.numpy as jnp
from jax import lax
from jax.sharding import PartitionSpec as P

KW = 31
norm_epsilon = 1e-05
residual_scale = 2.0**0.25


def norm_rows(values, gain_vector):
    row_mean = jnp.mean(values, axis=-1, keepdims=True)
    row_var = jnp.mean(jnp.square(values - row_mean), axis=-1, keepdims=True)
    return (values - row_mean) * lax.rsqrt(row_var + norm_epsilon) * gain_vector


def norm_shares(summed, stat_sums, full_width, gain_vector):
    row_mean = stat_sums[0] / full_width
    row_var = stat_sums[1] / full_width - row_mean * row_mean
    return (summed - row_mean[:, None]) * lax.rsqrt(row_var + norm_epsilon)[:, None] * gain_vector


def row_sums(summed):
    return (jnp.sum(summed, axis=1), jnp.sum(summed * summed, axis=1))


def contract(left, turned):
    return lax.dot_general(
        left, turned, (((1,), (1,)), ((), ())), preferred_element_type=jnp.float32
    )


def shards(
    stream,
    in_gain,
    value_weight,
    gate_weight,
    conv_kernel,
    conv_gain,
    conv_shift,
    out_weight,
    norm_gain,
    up_weight,
    down_weight,
    out_gain,
):
    seq_count, seq_length, model_width = stream.shape
    token_count = seq_count * seq_length
    tp_count = lax.axis_size("tp")
    slice_width = model_width // tp_count
    tp_index = lax.axis_index("tp")
    out_turned_shard = out_weight.T
    down_turned_shard = down_weight.T
    value_whole, gate_whole, out_turned, up_whole, down_turned = (
        lax.all_gather(value_weight, "fs", axis=0, tiled=True),
        lax.all_gather(gate_weight, "fs", axis=0, tiled=True),
        lax.all_gather(out_turned_shard, "fs", axis=0, tiled=True),
        lax.all_gather(up_weight, "fs", axis=0, tiled=True),
        lax.all_gather(down_turned_shard, "fs", axis=0, tiled=True),
    )
    normed = norm_rows(
        stream.reshape(token_count, model_width).astype(jnp.float32), in_gain
    ).astype(jnp.bfloat16)
    channels = value_weight.shape[1]
    values = jnp.dot(normed, value_whole, preferred_element_type=jnp.float32)
    gating = jnp.dot(normed, gate_whole, preferred_element_type=jnp.float32)
    gated = (values * jax.nn.sigmoid(gating)).astype(jnp.bfloat16)
    convolved = lax.conv_general_dilated(
        gated.reshape(seq_count, seq_length, channels),
        conv_kernel[:, None, :],
        window_strides=(1,),
        padding=[(KW - 1, 0)],
        dimension_numbers=("NWC", "WIO", "NWC"),
        feature_group_count=channels,
        preferred_element_type=jnp.float32,
    ).reshape(token_count, channels)
    conv_sums = lax.psum(row_sums(convolved), "tp")
    activated = jax.nn.silu(
        norm_shares(convolved, conv_sums, channels * tp_count, conv_gain) + conv_shift
    ).astype(jnp.bfloat16)
    partial_terms = contract(activated, out_turned)
    mixed = lax.psum_scatter(
        partial_terms.astype(jnp.bfloat16), "tp", scatter_dimension=1, tiled=True
    )
    normed_own = lax.dynamic_slice_in_dim(normed, tp_index * slice_width, slice_width, 1)
    gain_own = lax.dynamic_slice_in_dim(norm_gain, tp_index * slice_width, slice_width, 0)
    summed = residual_scale * normed_own.astype(jnp.float32) + mixed.astype(jnp.float32)
    mix_sums = lax.psum(row_sums(summed), "tp")
    settled_own = norm_shares(summed, mix_sums, model_width, gain_own).astype(jnp.bfloat16)
    settled_full = lax.all_gather(settled_own, "tp", axis=1, tiled=True)
    hidden = jnp.square(
        jax.nn.relu(jnp.dot(settled_full, up_whole, preferred_element_type=jnp.float32))
    ).astype(jnp.bfloat16)
    fed_terms = contract(hidden, down_turned)
    fed = lax.psum_scatter(fed_terms.astype(jnp.bfloat16), "tp", scatter_dimension=1, tiled=True)
    final_sum = residual_scale * settled_own.astype(jnp.float32) + fed.astype(jnp.float32)
    out_sums = lax.psum(row_sums(final_sum), "tp")
    result = norm_shares(final_sum, out_sums, model_width, out_gain).astype(jnp.bfloat16)
    return result.reshape(seq_count, seq_length, slice_width)


def solution(mesh):
    in_specs = (
        P(("grp", "fs"), None, None),
        P(),
        P("fs", "tp"),
        P("fs", "tp"),
        P(None, "tp"),
        P("tp"),
        P("tp"),
        P("tp", "fs"),
        P(),
        P("fs", "tp"),
        P("tp", "fs"),
        P("tp"),
    )
    out_specs = P(("grp", "fs"), None, "tp")
    return jax.shard_map(shards, mesh=mesh, in_specs=in_specs, out_specs=out_specs, check_vma=False)
```

profile of v0, /device:TPU:0, one launch (start us, length us, event | category | flops | bytes accessed | tf_op | source)
XLA Modules:
  0.0 465.8 jit_solution(17300026285777350739)
XLA Ops:
  8.8 1.2 convert_reduce_fusion
  10.0 1.3 fusion.11
  11.3 1.4 fusion.13
  12.8 26.9 %all-gather.6.cloned.1.call-done = bf16[2048,256]{1,0:T(8,128)(2,1)} async-done(((bf16[512,256]{1,0:T(8,128)(2,1)}), bf16[2048,256]{1,0:T(8,128)(2,1)}) %all-gather.6.cloned.1.call-update) | async-done | bytes 1048592 | tf_op jit(solution)/shard_map/all_gather | solution.py:55
  39.6 1.5 fusion.33
  41.2 27.4 %all-gather.8.cloned.1.call-done = bf16[2048,256]{1,0:T(8,128)(2,1)} async-done(((bf16[512,256]{1,0:T(8,128)(2,1)}), bf16[2048,256]{1,0:T(8,128)(2,1)}) %all-gather.8.cloned.1.call-update) | async-done | bytes 1048592 | tf_op jit(solution)/shard_map/all_gather | solution.py:56
  68.6 1.5 fusion.7
  70.2 2.2 fusion.32
  72.5 6.1 %all-reduce.2 = (f32[128]{0:T(128)S(1)}, f32[128]{0:T(128)S(1)}) all-reduce(f32[128]{0:T(128)S(1)} %fusion.21, f32[128]{0:T(128)S(1)} %get-tuple-element.21), channel_id=1, replica_groups=mesh['grp'=2,'fs'=4,'tp'=4] {'tp'}, use_global_device_ids=true, to_apply=%region_5.0 | all-reduce | flops 256 | bytes 2048 | tf_op jit(solution)/shard_map/psum | solution.py:77
  78.5 19.0 %all-gather.10.cloned.1.call-done = bf16[2048,256]{0,1:T(8,128)(2,1)} async-done(((bf16[512,256]{0,1:T(8,128)(2,1)}), bf16[2048,256]{0,1:T(8,128)(2,1)}) %all-gather.10.cloned.1.call-update) | async-done | bytes 1048592 | tf_op jit(solution)/shard_map/all_gather | solution.py:57
  97.6 2.4 convolution_convert_fusion.1
  101.2 0.8 dynamic_slice.7
  102.0 19.2 %reduce-scatter.3.cloned.1.call-done = bf16[128,512]{1,0:T(8,128)(2,1)} async-done(((bf16[128,2048]{1,0:T(8,128)(2,1)}), bf16[128,512]{1,0:T(8,128)(2,1)}) %reduce-scatter.3.cloned.1.call-update) | async-done | bytes 131088 | tf_op jit(solution)/shard_map/reduce_scatter | solution.py:82
  121.2 1.0 fusion.15
  122.2 5.8 %all-reduce.1 = (f32[128]{0:T(128)S(1)}, f32[128]{0:T(128)S(1)}) all-reduce(f32[128]{0:T(128)S(1)} %get-tuple-element.6, f32[128]{0:T(128)S(1)} %get-tuple-element.5), channel_id=1, replica_groups=mesh['grp'=2,'fs'=4,'tp'=4] {'tp'}, use_global_device_ids=true, to_apply=%region_10.11 | all-reduce | flops 256 | bytes 2048 | tf_op jit(solution)/shard_map/psum | solution.py:88
  128.0 1.0 multiply_convert_fusion.1
  129.0 6.9 %all_gather.21 = bf16[128,2048]{1,0:T(8,128)(2,1)S(1)} all-gather(bf16[128,512]{1,0:T(8,128)(2,1)S(1)} %multiply_convert_fusion.1), channel_id=1, replica_groups=mesh['grp'=2,'fs'=4,'tp'=4] {'tp'}, dimensions={1}, use_global_device_ids=true | all-gather | bytes 655360 | tf_op jit(solution)/shard_map/all_gather | solution.py:90
  135.9 136.3 %all-gather.12.cloned.1.call-done = bf16[2048,2048]{1,0:T(8,128)(2,1)} async-done(((bf16[512,2048]{1,0:T(8,128)(2,1)}), bf16[2048,2048]{1,0:T(8,128)(2,1)}) %all-gather.12.cloned.1.call-update) | async-done | bytes 8388624 | tf_op jit(solution)/shard_map/all_gather | solution.py:58
  272.2 149.3 %all-gather.14.cloned.1.call-done = bf16[2048,2048]{0,1:T(8,128)(2,1)} async-done(((bf16[512,2048]{0,1:T(8,128)(2,1)}), bf16[2048,2048]{0,1:T(8,128)(2,1)}) %all-gather.14.cloned.1.call-update) | async-done | bytes 8388624 | tf_op jit(solution)/shard_map/all_gather | solution.py:59
  421.5 8.9 %convolution_convert_fusion = bf16[128,2048]{1,0:T(8,128)(2,1)} fusion(bf16[2048,2048]{0,1:T(8,128)(2,1)} %all-gather.14.cloned.1.call-done, bf16[128,2048]{1,0:T(8,128)(2,1)S(1)} %all_gather.21, bf16[2048,2048]{1,0:T(8,128)(2,1)} %all-gather.12.cloned.1.call-done), kind=kOutput, calls=%fused_computation.2 | convolution fusion | flops 2148532224 | bytes 17825792 | tf_op jit(solution)/shard_map/dot_general | solution.py:28
  430.5 20.0 %reduce-scatter.5.cloned.1.call-done = bf16[128,512]{1,0:T(8,128)(2,1)} async-done(((bf16[128,2048]{1,0:T(8,128)(2,1)}), bf16[128,512]{1,0:T(8,128)(2,1)}) %reduce-scatter.5.cloned.1.call-update) | async-done | bytes 131088 | tf_op jit(solution)/shard_map/reduce_scatter | solution.py:95
  450.4 1.0 fusion.16
  451.5 5.8 %all-reduce = (f32[128]{0:T(128)S(1)}, f32[128]{0:T(128)S(1)}) all-reduce(f32[128]{0:T(128)S(1)} %get-tuple-element.8, f32[128]{0:T(128)S(1)} %get-tuple-element.7), channel_id=1, replica_groups=mesh['grp'=2,'fs'=4,'tp'=4] {'tp'}, use_global_device_ids=true, to_apply=%region_15.16 | all-reduce | flops 256 | bytes 2048 | tf_op jit(solution)/shard_map/psum | solution.py:97
  457.2 1.7 fusion.17
  (28 shorter events, 3.6 us)
Async XLA Ops:
  6.5 63.6 %copy-start = (bf16[31,256]{1,0:T(8,128)(2,1)S(1)}, bf16[31,256]{1,0:T(8,128)(2,1)}, u32[]{:S(2)}) copy-start(bf16[31,256]{1,0:T(8,128)(2,1)} %param.16) | copy-start | bytes 47620
  6.5 91.0 %copy-start.3 = (f32[256]{0:T(256)S(1)}, f32[256]{0:T(256)}, u32[]{:S(2)}) copy-start(f32[256]{0:T(256)} %param.17) | copy-start | bytes 3076
  6.5 91.0 %copy-start.2 = (f32[256]{0:T(256)S(1)}, f32[256]{0:T(256)}, u32[]{:S(2)}) copy-start(f32[256]{0:T(256)} %param.18) | copy-start | bytes 3076
  6.5 33.1 %all-gather.6.cloned.1.call-start = ((), (), s32[]{:S(2)}) async-start(), calls=%async_computation.2 | async-start | bytes 1310720 | tf_op jit(solution)/shard_map/all_gather | solution.py:55
  7.3 61.3 %all-gather.8.cloned.1.call-start = ((), (), s32[]{:S(2)}) async-start(), calls=%async_computation.3 | async-start | bytes 1310720 | tf_op jit(solution)/shard_map/all_gather | solution.py:56
  8.0 89.6 %all-gather.10.cloned.1.call-start = ((), (), s32[]{:S(2)}) async-start(), calls=%async_computation.4 | async-start | bytes 1310720 | tf_op jit(solution)/shard_map/all_gather | solution.py:57
  8.7 112.4 %reduce-scatter.3.cloned.1.call-start = ((), (), s32[]{:S(2)}) async-start(), calls=%async_computation.5 | async-start | bytes 655360 | tf_op jit(solution)/shard_map/reduce_scatter | solution.py:82
  100.0 172.2 %all-gather.12.cloned.1.call-start = ((), (), s32[]{:S(2)}) async-start(), calls=%async_computation.6 | async-start | bytes 10485760 | tf_op jit(solution)/shard_map/all_gather | solution.py:58
  100.6 320.9 %all-gather.14.cloned.1.call-start = ((), (), s32[]{:S(2)}) async-start(), calls=%async_computation.7 | async-start | bytes 10485760 | tf_op jit(solution)/shard_map/all_gather | solution.py:59
  101.2 349.2 %reduce-scatter.5.cloned.1.call-start = ((), (), s32[]{:S(2)}) async-start(), calls=%async_computation.8 | async-start | bytes 655360 | tf_op jit(solution)/shard_map/reduce_scatter | solution.py:95
  135.9 321.3 %copy-start.1 = (f32[512]{0:T(512)S(1)}, f32[512]{0:T(512)}, u32[]{:S(2)}) copy-start(f32[512]{0:T(512)} %param.23) | copy-start | bytes 6148
Sparse Core Ops, SparseCore 0:
  8.9 30.6 all-gather.5
  41.2 27.3 all-gather.7
  70.2 27.3 all-gather.9
  100.1 20.9 reduce-scatter.2
  122.6 149.6 all-gather.11
  273.7 147.7 all-gather.13
  430.6 19.7 reduce-scatter.4
where the time goes:
time: 466 us
  waiting for transfers between devices  401 us (86%)
  blocking collectives  24.5 us (5%)
  matrix products  16.6 us (4%)
  between operations  13.5 us (3%)
  other arithmetic  8.9 us (2%)
    all_gather x1, waiting for transfers between devices, shards(): lax.all_gather(down_turned_shard, 'fs', axis=0, tiled=True)  149 us
    all_gather x1, waiting for transfers between devices, shards(): lax.all_gather(up_weight, 'fs', axis=0, tiled=True)  136 us
    all_gather x1, waiting for transfers between devices, shards(): lax.all_gather(gate_weight, 'fs', axis=0, tiled=True)  27.4 us
    all_gather x1, waiting for transfers between devices, shards(): lax.all_gather(value_weight, 'fs', axis=0, tiled=True)  26.9 us
    reduce_scatter x1, waiting for transfers between devices, shards(): lax.psum_scatter(fed_terms.astype(jnp.bfloat16), 'tp', scatter_dimension=...  20 us
    reduce_scatter x1, waiting for transfers between devices, shards(): lax.psum_scatter(partial_terms.astype(jnp.bfloat16), 'tp', scatter_dimens...  19.2 us
    all_gather x1, waiting for transfers between devices, shards(): lax.all_gather(out_turned_shard, 'fs', axis=0, tiled=True)  19 us
    dot_general x2, matrix products, contract(): lax.dot_general(left, turned, (((1,), (1,)), ((), ())), preferred_element...  11.3 us
  transfers between devices with their start and end apart: 7, of which 7 were waited for; matrix products, arithmetic and copies ran while one was open for 3% of the time, Pallas kernels for 0%

commit v1 on v0

--- a/solution.py
+++ b/solution.py
@@ -6,6 +6,23 @@
 KW = 31
 norm_epsilon = 1e-05
 residual_scale = 2.0**0.25
+
+
+def in_order(tiles, dim):
+    tiles = jnp.moveaxis(tiles, 0, dim)
+    shape = tiles.shape
+    return tiles.reshape(*shape[:dim], shape[dim] * shape[dim + 1], *shape[dim + 2 :])
+
+
+def gather_around(shard, axis, dim):
+    length = lax.axis_size(axis)
+    forward = [(i, (i + 1) % length) for i in range(length)]
+    blocks = [shard]
+    while len(blocks) < length:
+        blocks.append(lax.ppermute(blocks[-1], axis, forward))
+    place = lax.axis_index(axis)
+    blocks = jnp.stack(blocks)[(place - jnp.arange(length)) % length]
+    return in_order(blocks, dim)
 
 
 def norm_rows(values, gain_vector):
@@ -52,7 +69,7 @@
     out_turned_shard = out_weight.T
     down_turned_shard = down_weight.T
     value_whole, gate_whole, out_turned, up_whole, down_turned = (
-        lax.all_gather(value_weight, "fs", axis=0, tiled=True),
+        gather_around(value_weight, "fs", 0),
         lax.all_gather(gate_weight, "fs", axis=0, tiled=True),
         lax.all_gather(out_turned_shard, "fs", axis=0, tiled=True),
         lax.all_gather(up_weight, "fs", axis=0, tiled=True),

time: 466 us -> 447 us (0.959)
  waiting for transfers between devices: 401 us -> 377 us
    ppermute x0 -> x3, waiting for transfers between devices: none -> 35.2 us  [gather_around(): blocks.append(lax.ppermute(blocks[-1], axis, forward))]
    all_gather x1, waiting for transfers between devices: 27.4 us -> 0.02 us  [shards(): lax.all_gather(gate_weight, 'fs', axis=0, tiled=True)]
    all_gather x1 -> x0, waiting for transfers between devices: 26.9 us -> none  [shards(): lax.all_gather(value_weight, 'fs', axis=0, tiled=True)]
    all_gather x1, waiting for transfers between devices: 136 us -> 149 us  [shards(): lax.all_gather(up_weight, 'fs', axis=0, tiled=True)]
    all_gather x1, waiting for transfers between devices: 149 us -> 136 us  [shards(): lax.all_gather(down_turned_shard, 'fs', axis=0, tiled=True)]
  transfers between devices with their start and end apart: 7 -> 9, of which waited for: 7 -> 8; matrix products, arithmetic and copies ran while one was open for 3% -> 3% of each run, Pallas kernels for 0% -> 0%
where the time goes in v1:
time: 447 us
  waiting for transfers between devices  377 us (84%)
  blocking collectives  24 us (5%)
  matrix products  16.4 us (4%)
  between operations  13.6 us (3%)
  other arithmetic  9.99 us (2%)
    all_gather x1, waiting for transfers between devices, shards(): lax.all_gather(up_weight, 'fs', axis=0, tiled=True)  149 us
    all_gather x1, waiting for transfers between devices, shards(): lax.all_gather(down_turned_shard, 'fs', axis=0, tiled=True)  136 us
    ppermute x3, waiting for transfers between devices, gather_around(): blocks.append(lax.ppermute(blocks[-1], axis, forward))  35.2 us
    reduce_scatter x1, waiting for transfers between devices, shards(): lax.psum_scatter(fed_terms.astype(jnp.bfloat16), 'tp', scatter_dimension=...  20 us
    reduce_scatter x1, waiting for transfers between devices, shards(): lax.psum_scatter(partial_terms.astype(jnp.bfloat16), 'tp', scatter_dimens...  19.2 us
    all_gather x1, waiting for transfers between devices, shards(): lax.all_gather(out_turned_shard, 'fs', axis=0, tiled=True)  15.2 us
    dot_general x2, matrix products, contract(): lax.dot_general(left, turned, (((1,), (1,)), ((), ())), preferred_element...  11.3 us
  transfers between devices with their start and end apart: 9, of which 8 were waited for; matrix products, arithmetic and copies ran while one was open for 3% of the time, Pallas kernels for 0%

profile of v1, /device:TPU:0, one launch (start us, length us, event | category | flops | bytes accessed | tf_op | source)
XLA Modules:
  0.0 446.8 jit_solution(12239456970679076502)
XLA Ops:
  7.3 3.1 collective-permute-start
  10.5 1.2 convert_reduce_fusion
  11.7 7.3 %collective-permute-done = bf16[512,256]{1,0:T(8,128)(2,1)S(1)} collective-permute-done((bf16[512,256]{1,0:T(8,128)(2,1)}, bf16[512,256]{1,0:T(8,128)(2,1)S(1)}, u32[]{:S(2)}, u32[]{:S(2)}) %collective-permute-start) | collective-permute-done | bytes 262176 | tf_op jit(solution)/shard_map/ppermute | solution.py:22
  19.0 1.3 fusion.11
  20.3 13.8 %collective-permute-done.1 = bf16[512,256]{1,0:T(8,128)(2,1)S(1)} collective-permute-done((bf16[512,256]{1,0:T(8,128)(2,1)S(1)}, bf16[512,256]{1,0:T(8,128)(2,1)S(1)}, u32[]{:S(2)}, u32[]{:S(2)}) %collective-permute-start.1) | collective-permute-done | bytes 262176 | tf_op jit(solution)/shard_map/ppermute | solution.py:22
  34.1 1.1 collective-permute-start.2
  35.1 1.4 fusion.13
  36.6 14.2 %collective-permute-done.2 = bf16[512,256]{1,0:T(8,128)(2,1)S(1)} collective-permute-done((bf16[512,256]{1,0:T(8,128)(2,1)S(1)}, bf16[512,256]{1,0:T(8,128)(2,1)S(1)}, u32[]{:S(2)}, u32[]{:S(2)}) %collective-permute-start.2) | collective-permute-done | bytes 262176 | tf_op jit(solution)/shard_map/ppermute | solution.py:22
  50.8 1.1 pad_maximum_fusion
  52.5 1.4 fusion.18
  53.9 1.6 fusion.7
  55.5 2.2 fusion.43
  57.8 5.7 %all-reduce.2 = (f32[128]{0:T(128)S(1)}, f32[128]{0:T(128)S(1)}) all-reduce(f32[128]{0:T(128)S(1)} %fusion.30, f32[128]{0:T(128)S(1)} %get-tuple-element.21), channel_id=1, replica_groups=mesh['grp'=2,'fs'=4,'tp'=4] {'tp'}, use_global_device_ids=true, to_apply=%region_5.6 | all-reduce | flops 256 | bytes 2048 | tf_op jit(solution)/shard_map/psum | solution.py:94
  63.5 15.2 %all-gather.7.cloned.1.call-done = bf16[2048,256]{0,1:T(8,128)(2,1)} async-done(((bf16[512,256]{0,1:T(8,128)(2,1)}), bf16[2048,256]{0,1:T(8,128)(2,1)}) %all-gather.7.cloned.1.call-update) | async-done | bytes 1048592 | tf_op jit(solution)/shard_map/all_gather | solution.py:74
  78.6 2.4 convolution_convert_fusion.1
  83.0 19.2 %reduce-scatter.3.cloned.1.call-done = bf16[128,512]{1,0:T(8,128)(2,1)} async-done(((bf16[128,2048]{1,0:T(8,128)(2,1)}), bf16[128,512]{1,0:T(8,128)(2,1)}) %reduce-scatter.3.cloned.1.call-update) | async-done | bytes 131088 | tf_op jit(solution)/shard_map/reduce_scatter | solution.py:99
  103.3 5.8 %all-reduce.1 = (f32[128]{0:T(128)S(1)}, f32[128]{0:T(128)S(1)}) all-reduce(f32[128]{0:T(128)S(1)} %get-tuple-element.6, f32[128]{0:T(128)S(1)} %get-tuple-element.5), channel_id=1, replica_groups=mesh['grp'=2,'fs'=4,'tp'=4] {'tp'}, use_global_device_ids=true, to_apply=%region_10.11 | all-reduce | flops 256 | bytes 2048 | tf_op jit(solution)/shard_map/psum | solution.py:105
  110.1 6.8 %all_gather.17 = bf16[128,2048]{1,0:T(8,128)(2,1)S(1)} all-gather(bf16[128,512]{1,0:T(8,128)(2,1)S(1)} %multiply_convert_fusion.1), channel_id=1, replica_groups=mesh['grp'=2,'fs'=4,'tp'=4] {'tp'}, dimensions={1}, use_global_device_ids=true | all-gather | bytes 655360 | tf_op jit(solution)/shard_map/all_gather | solution.py:107
  116.9 136.4 %all-gather.11.cloned.1.call-done = bf16[2048,2048]{0,1:T(8,128)(2,1)} async-done(((bf16[512,2048]{0,1:T(8,128)(2,1)}), bf16[2048,2048]{0,1:T(8,128)(2,1)}) %all-gather.11.cloned.1.call-update) | async-done | bytes 8388624 | tf_op jit(solution)/shard_map/all_gather | solution.py:76
  253.3 149.3 %all-gather.9.cloned.1.call-done = bf16[2048,2048]{1,0:T(8,128)(2,1)} async-done(((bf16[512,2048]{1,0:T(8,128)(2,1)}), bf16[2048,2048]{1,0:T(8,128)(2,1)}) %all-gather.9.cloned.1.call-update) | async-done | bytes 8388624 | tf_op jit(solution)/shard_map/all_gather | solution.py:75
  402.5 8.9 %convolution_convert_fusion = bf16[128,2048]{1,0:T(8,128)(2,1)} fusion(bf16[2048,2048]{0,1:T(8,128)(2,1)} %all-gather.11.cloned.1.call-done, bf16[128,2048]{1,0:T(8,128)(2,1)S(1)} %all_gather.17, bf16[2048,2048]{1,0:T(8,128)(2,1)} %all-gather.9.cloned.1.call-done), kind=kOutput, calls=%fused_computation.3 | convolution fusion | flops 2148532224 | bytes 17825792 | tf_op jit(solution)/shard_map/dot_general | solution.py:45
  411.5 20.0 %reduce-scatter.5.cloned.1.call-done = bf16[128,512]{1,0:T(8,128)(2,1)} async-done(((bf16[128,2048]{1,0:T(8,128)(2,1)}), bf16[128,512]{1,0:T(8,128)(2,1)}) %reduce-scatter.5.cloned.1.call-update) | async-done | bytes 131088 | tf_op jit(solution)/shard_map/reduce_scatter | solution.py:112
  432.5 5.8 %all-reduce = (f32[128]{0:T(128)S(1)}, f32[128]{0:T(128)S(1)}) all-reduce(f32[128]{0:T(128)S(1)} %get-tuple-element.8, f32[128]{0:T(128)S(1)} %get-tuple-element.7), channel_id=1, replica_groups=mesh['grp'=2,'fs'=4,'tp'=4] {'tp'}, use_global_device_ids=true, to_apply=%region_15.16 | all-reduce | flops 256 | bytes 2048 | tf_op jit(solution)/shard_map/psum | solution.py:114
  438.3 1.7 fusion.26
  (35 shorter events, 6.7 us)
Async XLA Ops:
  6.5 49.0 %copy-start = (bf16[31,256]{1,0:T(8,128)(2,1)S(1)}, bf16[31,256]{1,0:T(8,128)(2,1)}, u32[]{:S(2)}) copy-start(bf16[31,256]{1,0:T(8,128)(2,1)} %param.16) | copy-start | bytes 47620
  6.5 72.1 %copy-start.3 = (f32[256]{0:T(256)S(1)}, f32[256]{0:T(256)}, u32[]{:S(2)}) copy-start(f32[256]{0:T(256)} %param.17) | copy-start | bytes 3076
  6.5 72.1 %copy-start.2 = (f32[256]{0:T(256)S(1)}, f32[256]{0:T(256)}, u32[]{:S(2)}) copy-start(f32[256]{0:T(256)} %param.18) | copy-start | bytes 3076
  6.5 47.4 %all-gather.5.cloned.1.call-start = ((), (), s32[]{:S(2)}) async-start(), calls=%async_computation.2 | async-start | bytes 1310720 | tf_op jit(solution)/shard_map/all_gather | solution.py:73
  7.3 71.4 %all-gather.7.cloned.1.call-start = ((), (), s32[]{:S(2)}) async-start(), calls=%async_computation.3 | async-start | bytes 1310720 | tf_op jit(solution)/shard_map/all_gather | solution.py:74
  7.3 11.6 %collective-permute-start = (bf16[512,256]{1,0:T(8,128)(2,1)}, bf16[512,256]{1,0:T(8,128)(2,1)S(1)}, u32[]{:S(2)}, u32[]{:S(2)}) collective-permute-start(bf16[512,256]{1,0:T(8,128)(2,1)} %param.14), channel_id=1, source_target_pairs={{0,4},{4,8},{8,12},{12,0},{1,5},{5,9},{9,13},{13,1},{2,6},{6,10},{... | collective-permute-start | bytes 786440 | tf_op jit(solution)/shard_map/ppermute | solution.py:22
  10.4 91.8 %reduce-scatter.3.cloned.1.call-start = ((), (), s32[]{:S(2)}) async-start(), calls=%async_computation.4 | async-start | bytes 655360 | tf_op jit(solution)/shard_map/reduce_scatter | solution.py:99
  19.0 15.1 %collective-permute-start.1 = (bf16[512,256]{1,0:T(8,128)(2,1)S(1)}, bf16[512,256]{1,0:T(8,128)(2,1)S(1)}, u32[]{:S(2)}, u32[]{:S(2)}) collective-permute-start(bf16[512,256]{1,0:T(8,128)(2,1)S(1)} %collective-permute-done), channel_id=1, source_target_pairs={{0,4},{4,8},{8,12},{12,0},{1,5},{5,9},{9,13},{13,1},{2,6},{6,10},{... | collective-permute-start | bytes 786440 | tf_op jit(solution)/shard_map/ppermute | solution.py:22
  34.1 16.7 %collective-permute-start.2 = (bf16[512,256]{1,0:T(8,128)(2,1)S(1)}, bf16[512,256]{1,0:T(8,128)(2,1)S(1)}, u32[]{:S(2)}, u32[]{:S(2)}) collective-permute-start(bf16[512,256]{1,0:T(8,128)(2,1)S(1)} %collective-permute-done.1), channel_id=1, source_target_pairs={{0,4},{4,8},{8,12},{12,0},{1,5},{5,9},{9,13},{13,1},{2,6},{6,10},{... | collective-permute-start | bytes 786440 | tf_op jit(solution)/shard_map/ppermute | solution.py:22
  81.0 172.2 %all-gather.11.cloned.1.call-start = ((), (), s32[]{:S(2)}) async-start(), calls=%async_computation.6 | async-start | bytes 10485760 | tf_op jit(solution)/shard_map/all_gather | solution.py:76
  81.6 320.9 %all-gather.9.cloned.1.call-start = ((), (), s32[]{:S(2)}) async-start(), calls=%async_computation.5 | async-start | bytes 10485760 | tf_op jit(solution)/shard_map/all_gather | solution.py:75
  82.2 349.3 %reduce-scatter.5.cloned.1.call-start = ((), (), s32[]{:S(2)}) async-start(), calls=%async_computation.7 | async-start | bytes 655360 | tf_op jit(solution)/shard_map/reduce_scatter | solution.py:112
  116.9 321.4 %copy-start.1 = (f32[512]{0:T(512)S(1)}, f32[512]{0:T(512)}, u32[]{:S(2)}) copy-start(f32[512]{0:T(512)} %param.23) | copy-start | bytes 6148
Sparse Core Ops, SparseCore 0:
  8.9 41.9 all-gather.4
  52.4 26.1 all-gather.6
  81.2 20.9 reduce-scatter.2
  103.6 149.5 all-gather.10
  254.7 147.7 all-gather.8
  411.6 19.8 reduce-scatter.4
